TPU v7x, 32 devices: a whole 2x2x4 slice. The times are simulated.
32 devices in a mesh: grp: 2 (over y), sp: 4 (over z), tp: 4 (over x, core).
Axes of the slice: x: 2, y: 2, z: 4, core: 2. Of those that a mesh axis runs over, the one named last changes fastest.
Arguments:
- latent: bfloat16 [4096, 4096], P(('grp', 'sp'), 'tp'), parts along dimension 0, may hold values from -42 to 42
- context: bfloat16 [2048, 4096], P(('grp', 'sp'), 'tp'), parts along dimension 0, may hold values from -42 to 42
- conditions: float32 [4, 4096], P('grp', 'sp'), parts along dimension 0, may hold values from -6 to 6
- mod_weight: bfloat16 [4096, 3, 4096], P('sp', None, 'tp'), may hold values from -0.09375 to 0.09375
- norm_gain: float32 [4096], P('tp'), may hold values from 0.1 to 1.9
- w_query: bfloat16 [4096, 2048], P(None, 'tp'), may hold values from -0.09375 to 0.09375
- w_key: bfloat16 [4096, 2048], P(None, 'tp'), may hold values from -0.09375 to 0.09375
- w_value: bfloat16 [4096, 2048], P(None, 'tp'), may hold values from -0.09375 to 0.09375
- query_gain: float32 [64], replicated, may hold values from 1 to 14
- key_gain: float32 [64], replicated, may hold values from 1 to 14
- lambdas: float32 [16], P('tp'), may hold values from 0.3 to 0.8
- out_gain: float32 [128], replicated, may hold values from 0.1 to 1.9
- w_out: bfloat16 [2048, 4096], P(None, 'tp'), may hold values from -0.125 to 0.125
Outputs:
- updated: bfloat16 [4096, 4096], P(('grp', 'sp'), 'tp'), parts along dimension 0
There are 2 independent parts, one for each index of `grp`. A program takes and returns all parts, laid end to end along the dimension named above; an argument that names none is the same for every part. Nothing has to cross between parts.
All inputs are finite; a program needn't handle non-finite values.
Results may differ from a plain program's by a relative error of at most 0.0076.
Values may be sent and summed in bfloat16 or wider, within the bound.
A program may use at most 128 MiB of HBM per device.

v0:
```python
import math

import jax
import jax.numpy as jnp
from jax import lax
from jax.sharding import PartitionSpec as P

DK = 64
DV = 128
GRID_W = 64


epsilon = 1e-06


def turn_half(halves, angles):
    quarter = halves.shape[-1] // 2
    cosine = jnp.cos(angles)[:, None, None, :]
    sine_part = jnp.sin(angles)[:, None, None, :]
    first_part = halves[..., :quarter]
    second = halves[..., quarter:]
    return jnp.concatenate(
        [first_part * cosine - second * sine_part, first_part * sine_part + second * cosine],
        axis=-1,
    )


def rotate(features, positions):
    half_width = features.shape[-1] // 2
    quarter = half_width // 2
    inverse = 10000.0 ** (-2.0 * jnp.arange(quarter, dtype=jnp.float32) / half_width)
    grid_row = (positions // GRID_W).astype(jnp.float32)
    grid_column = (positions % GRID_W).astype(jnp.float32)
    return jnp.concatenate(
        [
            turn_half(features[..., :half_width], grid_row[:, None] * inverse),
            turn_half(features[..., half_width:], grid_column[:, None] * inverse),
        ],
        axis=-1,
    )


def head_norm(features, gain_row):
    return (
        features
        * lax.rsqrt(jnp.mean(features * features, axis=-1, keepdims=True) + epsilon)
        * gain_row
    )


def modulate(rows_in, gain_row, shift_row, scale_row):
    floats = rows_in.astype(jnp.float32)
    factor = lax.rsqrt(jnp.mean(floats * floats, axis=1, keepdims=True) + epsilon)
    return (floats * factor * gain_row * (1.0 + scale_row) + shift_row).astype(jnp.bfloat16)


def local(
    latent,
    context,
    conditions,
    mod_weight,
    norm_gain,
    w_query,
    w_key,
    w_value,
    query_gain,
    key_gain,
    lambdas,
    out_gain,
    w_out,
):
    tok_rows = latent.shape[0]
    ctx_rows = context.shape[0]
    columns = latent.shape[1]
    heads_here = lambdas.shape[0]
    in_rows = mod_weight.shape[0]
    activated = jax.nn.silu(conditions).astype(jnp.bfloat16)
    partial_mod = jnp.dot(
        activated, mod_weight.reshape(in_rows, 3 * columns), preferred_element_type=jnp.float32
    ).reshape(2, 3, columns)
    modulation = lax.psum(partial_mod, "sp")
    lat_floats = latent.astype(jnp.float32)
    full_gain, full_pairs = (
        lax.all_gather(norm_gain, "tp", axis=0, tiled=True),
        lax.all_gather(modulation[:, :2], "tp", axis=2, tiled=True),
    )
    whole_lat, whole_ctx = (
        lax.all_gather(latent, "tp", axis=1, tiled=True),
        lax.all_gather(context, "tp", axis=1, tiled=True),
    )
    hidden = modulate(whole_lat, full_gain, full_pairs[0, 0], full_pairs[0, 1])
    hidden_ctx = modulate(whole_ctx, full_gain, full_pairs[1, 0], full_pairs[1, 1])
    query_raw = jnp.dot(hidden, w_query, preferred_element_type=jnp.float32)
    key_raw = jnp.dot(hidden, w_key, preferred_element_type=jnp.float32)
    value_raw = jnp.dot(hidden, w_value, preferred_element_type=jnp.float32)
    ctx_key_raw = jnp.dot(hidden_ctx, w_key, preferred_element_type=jnp.float32)
    ctx_value_raw = jnp.dot(hidden_ctx, w_value, preferred_element_type=jnp.float32)
    positions = lax.axis_index("sp") * tok_rows + jnp.arange(tok_rows, dtype=jnp.int32)
    queries = rotate(
        head_norm(query_raw.reshape(tok_rows, heads_here, 2, DK), query_gain), positions
    ).astype(jnp.bfloat16)
    lat_keys = (
        rotate(head_norm(key_raw.reshape(tok_rows, heads_here, 2, DK), key_gain), positions)
        .astype(jnp.bfloat16)
        .reshape(tok_rows, heads_here * 2 * DK)
    )
    lat_values = value_raw.astype(jnp.bfloat16)
    ctx_keys = (
        head_norm(ctx_key_raw.reshape(ctx_rows, heads_here, 2, DK), key_gain)
        .astype(jnp.bfloat16)
        .reshape(ctx_rows, heads_here * 2 * DK)
    )
    ctx_values = ctx_value_raw.astype(jnp.bfloat16)
    scaling = DK ** (-0.5)

    def absorb(carried, key_rows, value_rows):
        key_count = key_rows.shape[0]
        key_block = key_rows.reshape(key_count, heads_here, 2, DK)
        value_block = value_rows.reshape(key_count, heads_here, DV)
        running_max, totals, weighted = carried
        scores = (
            jnp.einsum("qhmd,khmd->qhmk", queries, key_block, preferred_element_type=jnp.float32)
            * scaling
        )
        new_max = jnp.maximum(running_max, jnp.max(scores, axis=-1))
        rescale = jnp.exp(running_max - new_max)
        exponent = jnp.exp(scores - new_max[..., None])
        totals = totals * rescale + jnp.sum(exponent, axis=-1)
        weighted = weighted * rescale[..., None] + jnp.einsum(
            "qhmk,khv->qhmv",
            exponent.astype(jnp.bfloat16),
            value_block,
            preferred_element_type=jnp.float32,
        )
        return (new_max, totals, weighted)

    def absorb_rows(carried, key_rows, value_rows):
        key_count = key_rows.shape[0]
        block_rows = math.gcd(key_count, 512)

        def visit_block(block_index, partial_value):
            first_row = block_index * block_rows
            return absorb(
                partial_value,
                lax.dynamic_slice_in_dim(key_rows, first_row, block_rows, 0),
                lax.dynamic_slice_in_dim(value_rows, first_row, block_rows, 0),
            )

        return lax.fori_loop(0, key_count // block_rows, visit_block, carried)

    initial_state = (
        jnp.full((tok_rows, heads_here, 2), -1e30, jnp.float32),
        jnp.zeros((tok_rows, heads_here, 2), jnp.float32),
        jnp.zeros((tok_rows, heads_here, 2, DV), jnp.float32),
    )
    every_ctx_keys, every_ctx_values = (
        lax.all_gather(ctx_keys, "sp", axis=0, tiled=True),
        lax.all_gather(ctx_values, "sp", axis=0, tiled=True),
    )
    carried = absorb_rows(initial_state, every_ctx_keys, every_ctx_values)
    carried = absorb_rows(
        carried,
        lax.all_gather(lat_keys, "sp", axis=0, tiled=True),
        lax.all_gather(lat_values, "sp", axis=0, tiled=True),
    )
    running_max, totals, weighted = carried
    attended = (
        weighted[:, :, 0] / totals[:, :, 0, None]
        - lambdas[None, :, None] * weighted[:, :, 1] / totals[:, :, 1, None]
    )
    head_out = head_norm(attended, out_gain).astype(jnp.bfloat16).reshape(tok_rows, heads_here * DV)
    mixed_rows = jnp.dot(
        lax.all_gather(head_out, "tp", axis=1, tiled=True),
        w_out,
        preferred_element_type=jnp.float32,
    )
    return (lat_floats + modulation[0, 2] * mixed_rows).astype(jnp.bfloat16)


def solution(mesh):
    in_specs = (
        P(("grp", "sp"), "tp"),
        P(("grp", "sp"), "tp"),
        P("grp", "sp"),
        P("sp", None, "tp"),
        P("tp"),
        P(None, "tp"),
        P(None, "tp"),
        P(None, "tp"),
        P(),
        P(),
        P("tp"),
        P(),
        P(None, "tp"),
    )
    out_specs = P(("grp", "sp"), "tp")
    return jax.shard_map(local, mesh=mesh, in_specs=in_specs, out_specs=out_specs, check_vma=False)
```

profile of v0, /device:TPU:0, one launch (start us, length us, event | category | flops | bytes accessed | tf_op | source)
XLA Modules:
  0.0 294.6 jit_solution(11514742589361231051)
XLA Ops:
  8.8 8.6 %copy.31 = bf16[1024,3,1024]{0,2,1:T(8,128)(2,1)} copy(bf16[1024,3,1024]{2,0,1:T(8,128)(2,1)} %param.20) | data formatting | bytes 12582912 | tf_op args[3]
  17.5 5.1 %fusion.27 = f32[2,3,1024]{2,0,1:T(2,128)S(1)} fusion(bf16[1024,3,1024]{0,2,1:T(8,128)(2,1)} %copy.31, f32[2,1024]{1,0:T(2,128)S(1)} %copy-done.4), kind=kOutput, calls=%fused_computation.39 | convolution fusion | flops 12593152 | bytes 6324224 | tf_op jit(solution)/shard_map/dot_general | solution.py:78
  22.5 20.6 %psum.7 = f32[2,3,1024]{2,0,1:T(2,128)S(1)} all-reduce(f32[2,3,1024]{2,0,1:T(2,128)S(1)} %fusion.27), channel_id=1, replica_groups=mesh['grp'=2,'sp'=4,'tp'=4] {'sp'}, use_global_device_ids=true, to_apply=%region_0.1 | all-reduce | flops 6144 | bytes 49152 | tf_op jit(solution)/shard_map/psum | solution.py:81
  43.2 5.2 %all_gather.28 = f32[4096]{0:T(1024)S(1)} all-gather(f32[1024]{0:T(1024)S(1)} %copy-done.7), channel_id=1, replica_groups=mesh['grp'=2,'sp'=4,'tp'=4] {'tp'}, dimensions={0}, use_global_device_ids=true | all-gather | bytes 20480 | tf_op jit(solution)/shard_map/all_gather | solution.py:84
  48.4 5.6 %all_gather.29 = f32[2,2,4096]{2,0,1:T(2,128)S(1)} all-gather(f32[2,2,1024]{2,0,1:T(2,128)S(1)} %slice.85), channel_id=1, replica_groups=mesh['grp'=2,'sp'=4,'tp'=4] {'tp'}, dimensions={2}, use_global_device_ids=true | all-gather | bytes 81920 | tf_op jit(solution)/shard_map/all_gather | solution.py:85
  56.2 4.9 %convolution_convert_fusion.1 = bf16[256,512]{1,0:T(8,128)(2,1)} fusion(bf16[4096,512]{1,0:T(8,128)(2,1)} %param.24, bf16[256,4096]{1,0:T(8,128)(2,1)} %all-gather.8.cloned.1.call-done, f32[4096]{0:T(1024)S(1)} %bitcast.202, f32[4096]{0:T(1024)S(1)} %bitcast.204, f32[4096]{0:T(1024)S(1)} %all_gather.28, f32[256]{0:T(256)S(1)} %add_rsqrt_fusion.5), kind=kOutput, calls=%fused_computation.50 | convolution fusion | flops 1080164352 | bytes 6603776 | tf_op jit(solution)/shard_map/dot_general | solution.py:97
  61.4 5.0 %fusion.59 = (f32[256,512]{1,0:T(8,128)S(1)}, f32[256,512]{1,0:T(8,128)}) fusion(bf16[4096,512]{1,0:T(8,128)(2,1)} %param.23, bf16[256,4096]{1,0:T(8,128)(2,1)} %all-gather.8.cloned.1.call-done, f32[4096]{0:T(1024)S(1)} %bitcast.203, f32[4096]{0:T(1024)S(1)} %bitcast.205, f32[4096]{0:T(1024)S(1)} %all_gather.28, f32[256]{0:T(256)S(1)} %add_rsqrt_fusion.5), kind=kOutput, calls=%fused_computation.117 | convolution fusion | flops 1080164352 | bytes 7390208 | tf_op jit(solution)/shard_map/dot_general | solution.py:96
  70.7 3.2 %fusion.22 = f32[512]{0:T(512)S(1)} fusion(bf16[512,4096]{1,0:T(8,128)(2,1)} %all-gather.12.cloned.1.call-done), kind=kLoop, calls=%fused_computation.34 | loop fusion | flops 6290944 | bytes 4196352 | tf_op jit(solution)/shard_map/reduce_sum | solution.py:53
  74.1 5.4 %convolution_convert_fusion = bf16[512,512]{1,0:T(8,128)(2,1)} fusion(bf16[4096,512]{1,0:T(8,128)(2,1)} %param.24, bf16[512,4096]{1,0:T(8,128)(2,1)S(1)} %copy-done, f32[4096]{0:T(1024)S(1)} %bitcast.199, f32[4096]{0:T(1024)S(1)} %bitcast.196, f32[4096]{0:T(1024)S(1)} %all_gather.28, f32[512]{0:T(512)S(1)} %add_rsqrt_fusion.4), kind=kOutput, calls=%fused_computation.49 | convolution fusion | flops 2160328704 | bytes 8964096 | tf_op jit(solution)/shard_map/dot_general | solution.py:95
  79.8 6.4 %multiply_reduce_fusion = (f32[512,4,2]{0,2,1:T(2,128)S(1)}, f32[512,512]{0,1:T(8,128)S(1)}) fusion(bf16[4096,512]{1,0:T(8,128)(2,1)} %param.23, bf16[512,4096]{1,0:T(8,128)(2,1)} %all-gather.12.cloned.1.call-done, f32[4096]{0:T(1024)S(1)} %bitcast.200, f32[4096]{0:T(1024)S(1)} %bitcast.197, f32[4096]{0:T(1024)S(1)} %all_gather.28, f32[512]{0:T(512)S(1)} %add_rsqrt_fusion.4), kind=kOutput, calls=%fused_computation.64 | convolution fusion | flops 2160586752 | bytes 9504768 | tf_op jit(solution)/shard_map/dot_general | solution.py:94
  88.6 2.8 multiply_reduce_fusion.1
  92.2 8.0 %all-gather.14.cloned.1.call-done = bf16[1024,512]{1,0:T(8,128)(2,1)} async-done(((bf16[256,512]{1,0:T(8,128)(2,1)}), bf16[1024,512]{1,0:T(8,128)(2,1)}) %all-gather.14.cloned.1.call-update) | async-done | bytes 1048592 | tf_op jit(solution)/shard_map/all_gather | solution.py:158
  100.2 28.8 %all-gather.10.cloned.1.call-done = bf16[1024,512]{1,0:T(8,128)(2,1)} async-done(((bf16[256,512]{1,0:T(8,128)(2,1)}), bf16[1024,512]{1,0:T(8,128)(2,1)}) %all-gather.10.cloned.1.call-update) | async-done | bytes 1048592 | tf_op jit(solution)/shard_map/all_gather | solution.py:157
  129.0 20.6 %while.36 = (s32[]{:T(128)}, f32[512,4,2]{0,2,1:T(2,128)S(1)}, f32[512,4,2]{0,2,1:T(2,128)S(1)}, f32[512,4,2,128]{0,3,2,1:T(8,128)S(1)}, bf16[1024,512]{1,0:T(8,...) while((s32[]{:T(128)}, f32[512,4,2]{0,2,1:T(2,128)S(1)}, ...), condition=%wide.region_8.9_spmd.clone, body=%wide.region_5.8_spmd.clone.sunk | while | flops 823676928 | bytes 35389616 | solution.py:149
  133.3 2.4 bitcast_reduce_fusion.6
  137.2 2.1 bitcast_add_fusion.5
  143.7 2.4 bitcast_reduce_fusion.6
  147.5 2.1 bitcast_add_fusion.5
  149.7 25.8 %all-gather.18.cloned.1.call-done = bf16[2048,512]{1,0:T(8,128)(2,1)} async-done(((bf16[512,512]{1,0:T(8,128)(2,1)}), bf16[2048,512]{1,0:T(8,128)(2,1)}) %all-gather.18.cloned.1.call-update) | async-done | bytes 2097168 | tf_op jit(solution)/shard_map/all_gather | solution.py:164
  175.5 45.9 %all-gather.16.cloned.1.call-done = bf16[2048,512]{0,1:T(8,128)(2,1)} async-done(((bf16[512,512]{0,1:T(8,128)(2,1)}), bf16[2048,512]{0,1:T(8,128)(2,1)}) %all-gather.16.cloned.1.call-update) | async-done | bytes 2097168 | tf_op jit(solution)/shard_map/all_gather | solution.py:163
  221.4 36.4 %while.35 = (s32[]{:T(128)}, f32[512,4,2]{0,2,1:T(2,128)S(1)}, f32[512,4,2]{0,2,1:T(2,128)S(1)}, f32[512,4,2,128]{0,3,2,1:T(8,128)S(1)}, bf16[2048,512]{0,1:T(8,...) while((s32[]{:T(128)}, f32[512,4,2]{0,2,1:T(2,128)S(1)}, ...), condition=%wide.region_13.14_spmd, body=%wide.region_10.13_spmd.sunk | while | flops 823140352 | bytes 34341024 | solution.py:149
  237.5 2.1 bitcast_add_fusion.4
  260.8 20.8 %all-gather.20.cloned.1.call-done = bf16[512,2048]{0,1:T(8,128)(2,1)} async-done(((bf16[512,512]{0,1:T(8,128)(2,1)}), bf16[512,2048]{0,1:T(8,128)(2,1)}) %all-gather.20.cloned.1.call-update) | async-done | bytes 2097168 | tf_op jit(solution)/shard_map/all_gather | solution.py:173
  281.6 6.1 %add_convert_fusion = bf16[512,1024]{1,0:T(8,128)(2,1)} fusion(bf16[512,1024]{1,0:T(8,128)(2,1)S(1)} %copy-done.2, bf16[512,2048]{0,1:T(8,128)(2,1)} %all-gather.20.cloned.1.call-done, bf16[2048,1024]{1,0:T(8,128)(2,1)} %param.29, f32[1024]{0:T(1024)S(1)} %bitcast.206), kind=kOutput, calls=%fused_computation.48 | convolution fusion | flops 2149580800 | bytes 8392704 | tf_op jit(solution)/shard_map/dot_general | solution.py:172
  (131 shorter events, 61.1 us)
Async XLA Ops:
  6.5 47.5 %all-gather.8.cloned.1.call-start = ((), (), s32[]{:S(2)}) async-start(), calls=%async_computation | async-start | bytes 2621440 | tf_op jit(solution)/shard_map/all_gather | solution.py:89
  7.3 63.4 %all-gather.12.cloned.1.call-start = ((), (), s32[]{:S(2)}) async-start(), calls=%async_computation.2 | async-start | bytes 5242880 | tf_op jit(solution)/shard_map/all_gather | solution.py:88
  8.0 92.2 %all-gather.14.cloned.1.call-start = ((), (), s32[]{:S(2)}) async-start(), calls=%async_computation.3 | async-start | bytes 1310720 | tf_op jit(solution)/shard_map/all_gather | solution.py:158
  8.8 8.7 %copy-start.4 = (f32[2,1024]{1,0:T(2,128)S(1)}, f32[2,1024]{1,0:T(2,128)}, u32[]{:S(2)}) copy-start(f32[2,1024]{1,0:T(2,128)} %param.19) | copy-start | bytes 24580
  17.5 25.7 %copy-start.7 = (f32[1024]{0:T(1024)S(1)}, f32[1024]{0:T(1024)}, u32[]{:S(2)}) copy-start(f32[1024]{0:T(1024)} %param.21) | copy-start | bytes 12292
  43.1 17.9 %copy-start.3 = (f32[2,3,1024]{2,0,1:T(2,128)}, f32[2,3,1024]{2,0,1:T(2,128)S(1)}, u32[]{:S(2)}) copy-start(f32[2,3,1024]{2,0,1:T(2,128)S(1)} %psum.7) | copy-start | bytes 73732
  61.0 68.0 %all-gather.10.cloned.1.call-start = ((), (), s32[]{:S(2)}) async-start(), calls=%async_computation.1 | async-start | bytes 1310720 | tf_op jit(solution)/shard_map/all_gather | solution.py:157
  66.4 2.5 copy-start.9
  66.4 2.5 copy-start.12
  68.8 106.7 %all-gather.18.cloned.1.call-start = ((), (), s32[]{:S(2)}) async-start(), calls=%async_computation.5 | async-start | bytes 2621440 | tf_op jit(solution)/shard_map/all_gather | solution.py:164
  70.7 3.4 %copy-start = (bf16[512,4096]{1,0:T(8,128)(2,1)S(1)}, bf16[512,4096]{1,0:T(8,128)(2,1)}, u32[]{:S(2)}) copy-start(bf16[512,4096]{1,0:T(8,128)(2,1)} %all-gather.12.cloned.1.call-done) | copy-start | bytes 12582916
  79.5 6.7 %copy-start.8 = (f32[64]{0:T(128)S(1)}, f32[64]{0:T(128)}, u32[]{:S(2)}) copy-start(f32[64]{0:T(128)} %param.26) | copy-start | bytes 772
  79.5 141.9 %all-gather.16.cloned.1.call-start = ((), (), s32[]{:S(2)}) async-start(), calls=%async_computation.4 | async-start | bytes 2621440 | tf_op jit(solution)/shard_map/all_gather | solution.py:163
  79.8 7.7 %copy-start.13 = (bf16[4096,512]{1,0:T(8,128)(2,1)S(1)}, bf16[4096,512]{1,0:T(8,128)(2,1)}, u32[]{:S(2)}) copy-start(bf16[4096,512]{1,0:T(8,128)(2,1)} %param.22) | copy-start | bytes 12582916
  86.2 2.4 copy-start.1
  88.6 2.8 copy-start.11
  91.9 189.7 %all-gather.20.cloned.1.call-start = ((), (), s32[]{:S(2)}) async-start(), calls=%async_computation.6 | async-start | bytes 2621440 | tf_op jit(solution)/shard_map/all_gather | solution.py:173
  257.9 0.7 copy-start.10
  258.0 1.0 copy-start.5
  258.0 1.0 copy-start.6
  258.2 23.4 %copy-start.2 = (bf16[512,1024]{1,0:T(8,128)(2,1)S(1)}, bf16[512,1024]{1,0:T(8,128)(2,1)}, u32[]{:S(2)}) copy-start(bf16[512,1024]{1,0:T(8,128)(2,1)} %param.17) | copy-start | bytes 3145732
Sparse Core Ops, SparseCore 0:
  8.9 25.2 all-gather.7
  35.8 34.8 all-gather.11
  72.3 27.8 all-gather.13
  101.6 27.3 all-gather.9
  130.4 45.0 all-gather.17
  176.9 44.4 all-gather.15
  260.2 21.3 all-gather.19
where the time goes:
time: 296 us; the launch traced here: 295 us
  waiting for transfers between devices  132 us (45%)
  matrix products  58.2 us (20%)
  local copies, waits for them, and re-layouts  38.6 us (13%)
  blocking collectives  31.4 us (11%)
  other arithmetic  19.5 us (7%)
  between operations  13.9 us (5%)
    all_gather x1, waiting for transfers between devices, local(): lax.all_gather(lat_keys, 'sp', axis=0, tiled=True)  45.9 us
    all_gather x1, waiting for transfers between devices, local(): lax.all_gather(ctx_keys, 'sp', axis=0, tiled=True)  28.8 us
    all_gather x1, waiting for transfers between devices, local(): lax.all_gather(lat_values, 'sp', axis=0, tiled=True)  25.8 us
    all_gather x1, waiting for transfers between devices, local(): lax.all_gather(head_out, 'tp', axis=1, tiled=True)  20.8 us
    psum x1, blocking collectives, local(): modulation = lax.psum(partial_mod, 'sp')  20.6 us
    dynamic_slice x12, local copies, waits for them, and re-layouts, visit_block(): lax.dynamic_slice_in_dim(value_rows, first_row, block_rows, 0)  19.1 us
    dot_general x6, matrix products, absorb(): jnp.einsum('qhmk,khv->qhmv', exponent.astype(jnp.bfloat16), value_block,...  12.7 us
    unnamed x31, local copies, waits for them, and re-layouts  10.2 us
  transfers between devices with their start and end apart: 7, of which 6 were waited for; matrix products, arithmetic and copies ran while one was open for 24% of the time, Pallas kernels for 0%

commit v1 on v0

--- a/solution.py
+++ b/solution.py
@@ -1,8 +1,11 @@
+import functools
 import math
 
 import jax
 import jax.numpy as jnp
 from jax import lax
+from jax.experimental import pallas as pl
+from jax.experimental.pallas import tpu as pltpu
 from jax.sharding import PartitionSpec as P
 
 DK = 64
@@ -54,7 +57,7 @@
     return (floats * factor * gain_row * (1.0 + scale_row) + shift_row).astype(jnp.bfloat16)
 
 
-def local(
+def plain(
     latent,
     context,
     conditions,
@@ -177,6 +180,385 @@
     return (lat_floats + modulation[0, 2] * mixed_rows).astype(jnp.bfloat16)
 
 
+MESH = pl.DeviceIdType.MESH
+BF = jnp.bfloat16
+F32 = jnp.float32
+
+
+def fused_kernel(
+    sp, tp, lat, ctx, part, gain, wq_h, wk_h, wv_h, wo_h, qc, qs, kc, ks, ckg, lam, og, ones_bd,
+    out, X, PA, CO, WQ, WK, WV, WO, H, SL, SC, RL, RC, KX, VX, SS, OS, HO,
+    loc_sem, w_sem, xs, xr, ds, dr, fs, fr, ps, pr, cs, cr, zs, zr, os_, or_, gs, gr, es, er, hs, hr,
+):
+    ms = lax.axis_index("sp")
+    mt = lax.axis_index("tp")
+    nx = tp // 2
+    core = lax.rem(mt, 2)
+    base = mt - core
+    mate = base + 1 - core
+    xp = [lax.rem(base + 2 * d, tp) + core for d in range(1, nx)]
+    xq = [lax.rem(base + tp - 2 * d, tp) + core for d in range(1, nx)]
+    xqm = [lax.rem(base + tp - 2 * d, tp) + 1 - core for d in range(1, nx)]
+    zp = [lax.rem(ms + d, sp) for d in range(1, sp)]
+    zq = [lax.rem(ms + sp - d, sp) for d in range(1, sp)]
+    tpn = [lax.rem(mt + d, tp) for d in range(1, tp)]
+    tpq = [lax.rem(mt + tp - d, tp) for d in range(1, tp)]
+    n = ctx.shape[0]
+    cols = lat.shape[1]
+    nl = lat.shape[0] // n
+
+    barrier = pltpu.get_barrier_semaphore()
+    for p in zp:
+        pl.semaphore_signal(barrier, inc=1, device_id={"sp": p}, device_id_type=MESH)
+    for p in tpn:
+        pl.semaphore_signal(barrier, inc=1, device_id={"tp": p}, device_id_type=MESH)
+
+    def local_in(c):
+        src = ctx if c == 0 else lat.at[pl.ds((c - 1) * n, n)]
+        return pltpu.make_async_copy(src, X.at[mt, pl.ds(c * n, n)], loc_sem.at[c])
+
+    for c in range(nl + 1):
+        local_in(c).start()
+    weights = [
+        pltpu.make_async_copy(a, b, w_sem.at[i])
+        for i, (a, b) in enumerate(((wk_h, WK), (wv_h, WV), (wq_h, WQ), (wo_h, WO)))
+    ]
+    for w in weights:
+        w.start()
+    pl.semaphore_wait(barrier, (sp - 1) + (tp - 1))
+
+    def remote(src, dst, ssem, rsem, where):
+        return pltpu.make_async_remote_copy(
+            src_ref=src, dst_ref=dst, send_sem=ssem, recv_sem=rsem,
+            device_id=where, device_id_type=MESH,
+        )
+
+    def source(c):
+        return ctx if c == 0 else lat.at[pl.ds((c - 1) * n, n)]
+
+    def x_send(c, d):
+        return remote(source(c), X.at[mt, pl.ds(c * n, n)], xs.at[c, d], xr.at[c, d], {"tp": xp[d]})
+
+    def d_send(c):
+        return remote(source(c), X.at[mt, pl.ds(c * n, n)], ds.at[c], dr.at[c], {"tp": mate})
+
+    def p_send(d):
+        return remote(part, PA.at[ms], ps.at[d], pr.at[d], {"sp": zp[d]})
+
+    def c_send(d):
+        return remote(CO.at[mt], CO.at[mt], cs.at[d], cr.at[d], {"tp": tpn[d]})
+
+    for d in range(sp - 1):
+        p_send(d).start()
+    for d in range(nx - 1):
+        x_send(0, d).start()
+    for c in range(nl + 1):
+        d_send(c).start()
+
+    PA[ms] = part[...]
+    for d in range(sp - 1):
+        p_send(d).wait()
+    total = PA[0]
+    for s in range(1, sp):
+        total = total + PA[s]
+    CO[mt, 0:1, :] = gain[...] * (1.0 + total[1:2])
+    CO[mt, 1:2, :] = total[0:1]
+    CO[mt, 2:3, :] = gain[...] * (1.0 + total[4:5])
+    CO[mt, 3:4, :] = total[3:4]
+    CO[mt, 4:5, :] = total[2:3]
+    CO[mt, 5:8, :] = jnp.zeros((3, cols), F32)
+    for d in range(tp - 1):
+        c_send(d).start()
+    for c in range(1, nl + 1):
+        for d in range(nx - 1):
+            x_send(c, d).start()
+    for d in range(tp - 1):
+        c_send(d).wait()
+
+    lane = lax.broadcasted_iota(jnp.int32, (n, 2 * DK), 1)
+    low = lax.rem(lane, DK // 2) < DK // 4
+
+    def f_send(c, d):
+        ref = X.at[xq[d], pl.ds(c * n, n)]
+        return remote(ref, ref, fs.at[c, d], fr.at[c, d], {"tp": mate})
+
+    def z_send(c, d):
+        if c == 0:
+            return remote(SC.at[zp[d]], RC.at[ms], zs.at[c, d], zr.at[c, d], {"sp": zp[d]})
+        return remote(
+            SL.at[zp[d], c - 1], RL.at[ms, c - 1], zs.at[c, d], zr.at[c, d], {"sp": zp[d]}
+        )
+
+    def normed(v):
+        square = (v * v).astype(BF)
+        mean = jnp.dot(square, ones_bd[...], preferred_element_type=F32)
+        return v * lax.rsqrt(mean * (1.0 / DK) + epsilon)
+
+    def turned(v, ctab, stab):
+        w = normed(v)
+        swapped = jnp.where(low, pltpu.roll(w, 2 * DK - DK // 4, 1), pltpu.roll(w, DK // 4, 1))
+        return (w * ctab + swapped * stab).astype(BF)
+
+    for c in range(nl + 1):
+        rows = pl.ds(c * n, n)
+        local_in(c).wait()
+        for d in range(nx - 1):
+            x_send(c, d).wait()
+            f_send(c, d).start()
+        d_send(c).wait()
+        for d in range(nx - 1):
+            f_send(c, d).wait()
+        ss = jnp.zeros((n, 1), F32)
+        for t in range(tp):
+            f = X[t, rows, :].astype(F32)
+            ss = ss + jnp.sum(f * f, axis=1, keepdims=True)
+        factor = lax.rsqrt(ss * (1.0 / (tp * cols)) + epsilon)
+        r0 = 2 if c == 0 else 0
+        for t in range(tp):
+            f = X[t, rows, :].astype(F32)
+            co = CO[t]
+            H[:, t * cols:(t + 1) * cols] = (
+                f * factor * co[r0:r0 + 1] + co[r0 + 1:r0 + 2]
+            ).astype(BF)
+        if c == 0:
+            weights[0].wait()
+            weights[1].wait()
+        if c == 1:
+            weights[2].wait()
+        off = 0 if c == 0 else DV
+        if c > 0:
+            tr = pl.ds((c - 1) * n, n)
+            raw = jnp.dot(H[...], WQ[...], preferred_element_type=F32)
+            for z in range(sp):
+                SL[z, c - 1, :, 0:DV] = turned(raw[:, z * DV:(z + 1) * DV], qc[tr, :], qs[tr, :])
+        raw = jnp.dot(H[...], WK[...], preferred_element_type=F32)
+        for z in range(sp):
+            piece = raw[:, z * DV:(z + 1) * DV]
+            if c == 0:
+                SC[z, :, 0:DV] = (normed(piece) * ckg[...]).astype(BF)
+            else:
+                SL[z, c - 1, :, DV:2 * DV] = turned(piece, kc[tr, :], ks[tr, :])
+        raw = jnp.dot(H[...], WV[...], preferred_element_type=F32)
+        for z in range(sp):
+            piece = raw[:, z * DV:(z + 1) * DV].astype(BF)
+            if c == 0:
+                SC[z, :, DV:2 * DV] = piece
+            else:
+                SL[z, c - 1, :, 2 * DV:3 * DV] = piece
+        for d in range(sp - 1):
+            z_send(c, d).start()
+        if c == 0:
+            RC[ms] = SC[ms]
+        else:
+            RL[ms, c - 1] = SL[ms, c - 1]
+
+    for c in range(nl + 1):
+        for d in range(sp - 1):
+            z_send(c, d).wait()
+    nk = sp * (nl + 1)
+    for s in range(sp):
+        for c in range(nl + 1):
+            kb = s * (nl + 1) + c
+            if c == 0:
+                KX[kb] = RC[s, :, 0:DV]
+                VX[kb, :, 0:DV] = RC[s, :, DV:2 * DV]
+            else:
+                KX[kb] = RL[s, c - 1, :, DV:2 * DV]
+                VX[kb, :, 0:DV] = RL[s, c - 1, :, 2 * DV:3 * DV]
+            VX[kb, :, DV:2 * DV] = jnp.ones((n, DV), BF)
+
+    first = lane < DK
+
+    def o_send(half, d):
+        return remote(
+            OS.at[half, zp[d]],
+            HO.at[mt, pl.ds(half * n, n), pl.ds(pl.multiple_of(ms * DV, DV), DV)],
+            os_.at[half, d], or_.at[half, d], {"sp": zp[d]},
+        )
+
+    def g_send(half, d):
+        ref = HO.at[mt, pl.ds(half * n, n)]
+        return remote(ref, ref, gs.at[half, d], gr.at[half, d], {"tp": xp[d]})
+
+    def e_send(half):
+        ref = HO.at[mt, pl.ds(half * n, n)]
+        return remote(ref, ref, es.at[half], er.at[half], {"tp": mate})
+
+    def h_send(half, d):
+        ref = HO.at[xq[d], pl.ds(half * n, n)]
+        return remote(ref, ref, hs.at[half, d], hr.at[half, d], {"tp": mate})
+
+    def attend(z, half):
+        q = RL[z, half, :, 0:DV]
+        zero = jnp.zeros_like(q)
+        qq = jnp.concatenate([jnp.where(first, q, zero), jnp.where(first, zero, q)], axis=0)
+        peak = None
+        for kb in range(nk):
+            s = lax.dot_general(qq, KX[kb], (((1,), (1,)), ((), ())), preferred_element_type=F32)
+            SS[kb] = s
+            for j in range(n // 128):
+                piece = s[:, j * 128:(j + 1) * 128]
+                peak = piece if peak is None else jnp.maximum(peak, piece)
+        peak = jnp.max(peak, axis=1, keepdims=True)
+        acc = jnp.zeros((2 * n, 2 * DV), F32)
+        for kb in range(nk):
+            p = jnp.exp2(SS[kb] - peak).astype(BF)
+            acc = acc + jnp.dot(p, VX[kb], preferred_element_type=F32)
+        o = acc[:, :DV] / acc[:, DV:]
+        a = o[:n] - lam[...] * o[n:]
+        a = a * lax.rsqrt(jnp.mean(a * a, axis=1, keepdims=True) + epsilon) * og[...]
+        return a.astype(BF)
+
+    for half in range(nl):
+        def step(i, carry):
+            z = lax.rem(ms + 1 + i, sp)
+            OS[half, z] = attend(z, half)
+            for d in range(sp - 1):
+                @pl.when(i == d)
+                def _():
+                    o_send(half, d).start()
+            return carry
+
+        lax.fori_loop(0, sp, step, 0)
+        HO[mt, half * n:(half + 1) * n, pl.ds(pl.multiple_of(ms * DV, DV), DV)] = OS[half, ms]
+        for d in range(sp - 1):
+            o_send(half, d).wait()
+        for d in range(nx - 1):
+            g_send(half, d).start()
+        e_send(half).start()
+
+    weights[3].wait()
+    width = sp * DV
+    for half in range(nl):
+        for d in range(nx - 1):
+            g_send(half, d).wait()
+            h_send(half, d).start()
+        e_send(half).wait()
+        for d in range(nx - 1):
+            h_send(half, d).wait()
+        rows = slice(half * n, (half + 1) * n)
+        mixed = jnp.zeros((n, cols), F32)
+        for t in range(tp):
+            mixed = mixed + jnp.dot(
+                HO[t, rows, :], WO[t * width:(t + 1) * width, :], preferred_element_type=F32
+            )
+        residual = X[mt, pl.ds(n + half * n, n), :].astype(F32)
+        out[rows, :] = (residual + CO[mt, 4:5, :] * mixed).astype(BF)
+
+
+def swap_lanes(v):
+    quarter = DK // 4
+    return jnp.concatenate(
+        [
+            v[..., quarter:2 * quarter], v[..., :quarter],
+            v[..., 3 * quarter:], v[..., 2 * quarter:3 * quarter],
+        ],
+        axis=-1,
+    )
+
+
+def fused(
+    sp, tp, latent, context, conditions, mod_weight, norm_gain, w_query, w_key, w_value,
+    query_gain, key_gain, lambdas, out_gain, w_out,
+):
+    tok, cols = latent.shape
+    n = context.shape[0]
+    nl = tok // n
+    activated = jax.nn.silu(conditions).astype(BF).astype(F32)
+    weight = mod_weight.astype(F32)
+    part = jnp.concatenate(
+        [jnp.sum(weight * activated[c][:, None, None], axis=0) for c in range(2)]
+        + [jnp.zeros((2, cols), F32)],
+        axis=0,
+    )
+    positions = lax.axis_index("sp") * tok + jnp.arange(tok, dtype=jnp.int32)
+    quarter = DK // 4
+    inverse = 10000.0 ** (-4.0 * jnp.arange(quarter, dtype=F32) / DK)
+    row_angle = (positions // GRID_W).astype(F32)[:, None] * inverse
+    column_angle = (positions % GRID_W).astype(F32)[:, None] * inverse
+    cosine = jnp.concatenate([jnp.cos(row_angle)] * 2 + [jnp.cos(column_angle)] * 2, axis=1)
+    rs, cs = jnp.sin(row_angle), jnp.sin(column_angle)
+    sine = jnp.concatenate([-rs, rs, -cs, cs], axis=1)
+    factor = DK ** (-0.5) * math.log2(math.e)
+
+    def pair(g, scale):
+        c = cosine * (g * scale)
+        s = sine * (swap_lanes(g) * scale)
+        return jnp.concatenate([c, c], axis=1), jnp.concatenate([s, s], axis=1)
+
+    qc, qs = pair(query_gain, factor)
+    kc, ks = pair(key_gain, 1.0)
+    ckg = jnp.concatenate([key_gain, key_gain])[None]
+    lam = jnp.broadcast_to(
+        lax.dynamic_slice_in_dim(lambdas, lax.axis_index("sp"), 1)[None], (1, DV)
+    )
+    which = jnp.arange(2 * DK) // DK
+    ones_bd = (which[:, None] == which[None]).astype(BF)
+    nx = tp // 2
+    any_ = pl.BlockSpec(memory_space=pl.ANY)
+    vm = pl.BlockSpec(memory_space=pltpu.VMEM)
+    dma = pltpu.SemaphoreType.DMA
+    kdim, wcols = w_query.shape
+    nk = sp * (nl + 1)
+    return pl.pallas_call(
+        functools.partial(fused_kernel, sp, tp),
+        out_shape=jax.ShapeDtypeStruct((tok, cols), BF),
+        in_specs=[any_, any_, vm, vm, any_, any_, any_, any_] + [vm] * 8,
+        out_specs=vm,
+        scratch_shapes=[
+            pltpu.VMEM((tp, n + tok, cols), BF),
+            pltpu.VMEM((sp, 8, cols), F32),
+            pltpu.VMEM((tp, 8, cols), F32),
+            pltpu.VMEM((kdim, wcols), BF),
+            pltpu.VMEM((kdim, wcols), BF),
+            pltpu.VMEM((kdim, wcols), BF),
+            pltpu.VMEM(w_out.shape, BF),
+            pltpu.VMEM((n, kdim), BF),
+            pltpu.VMEM((sp, nl, n, 3 * DV), BF),
+            pltpu.VMEM((sp, n, 2 * DV), BF),
+            pltpu.VMEM((sp, nl, n, 3 * DV), BF),
+            pltpu.VMEM((sp, n, 2 * DV), BF),
+            pltpu.VMEM((nk, n, DV), BF),
+            pltpu.VMEM((nk, n, 2 * DV), BF),
+            pltpu.VMEM((nk, 2 * n, n), F32),
+            pltpu.VMEM((nl, sp, n, DV), BF),
+            pltpu.VMEM((tp, tok, sp * DV), BF),
+            dma((nl + 1,)),
+            dma((4,)),
+            dma((nl + 1, nx - 1)), dma((nl + 1, nx - 1)),
+            dma((nl + 1,)), dma((nl + 1,)),
+            dma((nl + 1, nx - 1)), dma((nl + 1, nx - 1)),
+            dma((sp - 1,)), dma((sp - 1,)),
+            dma((tp - 1,)), dma((tp - 1,)),
+            dma((nl + 1, sp - 1)), dma((nl + 1, sp - 1)),
+            dma((nl, sp - 1)), dma((nl, sp - 1)),
+            dma((nl, nx - 1)), dma((nl, nx - 1)),
+            dma((nl,)), dma((nl,)),
+            dma((nl, nx - 1)), dma((nl, nx - 1)),
+        ],
+        compiler_params=pltpu.CompilerParams(
+            collective_id=0, has_side_effects=True, vmem_limit_bytes=60 * 1024 * 1024
+        ),
+    )(
+        latent, context, part, norm_gain[None], w_query, w_key, w_value, w_out,
+        qc, qs, kc, ks, ckg, lam, out_gain[None], ones_bd,
+    )
+
+
+def local(sp, tp, *arguments):
+    latent, context, lambdas = arguments[0], arguments[1], arguments[10]
+    rows = context.shape[0]
+    fits = (
+        lambdas.shape[0] == sp and sp > 1 and tp % 2 == 0 and tp > 2
+        and latent.shape[0] % rows == 0 and rows % 128 == 0 and rows <= 256
+        and latent.shape[0] <= 2 * rows and latent.shape[1] % 128 == 0
+        and latent.shape[1] <= 1024 and tp <= 4
+    )
+    if fits:
+        return fused(sp, tp, *arguments)
+    return plain(*arguments)
+
+
 def solution(mesh):
     in_specs = (
         P(("grp", "sp"), "tp"),
@@ -194,4 +576,5 @@
         P(None, "tp"),
     )
     out_specs = P(("grp", "sp"), "tp")
-    return jax.shard_map(local, mesh=mesh, in_specs=in_specs, out_specs=out_specs, check_vma=False)
+    body = functools.partial(local, mesh.shape["sp"], mesh.shape["tp"])
+    return jax.shard_map(body, mesh=mesh, in_specs=in_specs, out_specs=out_specs, check_vma=False)

time: 296 us -> 135 us (0.46)
  waiting for transfers between devices: 132 us -> 0 us
  Pallas kernels: 0 us -> 115 us
  matrix products: 58.2 us -> 0 us
  local copies, waits for them, and re-layouts: 38.6 us -> 5.86 us
  blocking collectives: 31.4 us -> 0 us
  between operations: 13.9 us -> 0.09 us
  other arithmetic: 19.5 us -> 14.5 us
    all_gather x7 -> x0, waiting for transfers between devices: 131 us -> none  [the longest x1 45.9 us: local(): lax.all_gather(lat_keys, 'sp', axis=0, tiled=True)]
    pallas_call x0 -> x1, Pallas kernels: none -> 115 us  [fused(): pl.pallas_call(functools.partial(fused_kernel, sp, tp), out_shape=jax.Sha...]
    dot_general x19 -> x0, matrix products: 58.2 us -> none  [the longest x6 12.7 us: absorb(): jnp.einsum('qhmk,khv->qhmv', exponent.astype(jnp.bfloat16), value_block,...]
    dynamic_slice x18 -> x1, local copies, waits for them, and re-layouts: 25.5 us -> 0.59 us  [fused(): lax.dynamic_slice_in_dim(lambdas, lax.axis_index('sp'), 1)[None]]
    psum x1 -> x0, blocking collectives: 20.6 us -> none  [local(): modulation = lax.psum(partial_mod, 'sp')]
    all_gather x2 -> x0, blocking collectives: 10.8 us -> none  [the longest x1 5.6 us: local(): lax.all_gather(modulation[:, :2], 'tp', axis=2, tiled=True)]
    reduce_sum x10 -> x1, other arithmetic: 14.1 us -> 5.12 us  [fused(): jnp.sum(weight * activated[c][:, None, None], axis=0)]
    unnamed x31 -> x7, local copies, waits for them, and re-layouts: 10.2 us -> 2.28 us
  transfers between devices with their start and end apart: 7 -> 0, of which waited for: 6 -> 0; matrix products, arithmetic and copies ran while one was open for 24% -> 0% of each run, Pallas kernels for 0% -> 0%
where the time goes in v1:
time: 135 us
  Pallas kernels  115 us (85%)
  other arithmetic  14.5 us (11%)
  local copies, waits for them, and re-layouts  5.86 us (4%)
    pallas_call x1, Pallas kernels, fused(): pl.pallas_call(functools.partial(fused_kernel, sp, tp), out_shape=jax.Sha...  115 us
    reduce_sum x1, other arithmetic, fused(): jnp.sum(weight * activated[c][:, None, None], axis=0)  5.12 us
    concatenate x4, other arithmetic, pair(): return (jnp.concatenate([c, c], axis=1), jnp.concatenate([s, s], axis=1))  3.35 us

profile of v1, /device:TPU:0, one launch (start us, length us, event | category | flops | bytes accessed | tf_op | source)
XLA Modules:
  0.0 135.0 jit_solution(11599489594572816170)
XLA Ops:
  0.0 0.0 copy-start
  0.0 1.9 %fusion.2 = (f32[512,16]{1,0:T(8,128)S(1)}, f32[512,16]{1,0:T(8,128)S(1)}, f32[512,16]{1,0:T(8,128)S(1)}, f32[512,16]{1,0:T(8,128)S(1)}, f32[512,16]{1,0:T(8,128)S(1)}, /*index=5*/f32[512,16]{1,0:T(8,128)S(1)}) fusion(f32[16]{0:T(128)S(1)} %multiply_power_fusion, f32[512]{0:T(512)S(1)} %get-tuple-element.30, f32[512]{0:T(512)S(1)} %get-tuple-element.31), kind=kLoop, calls=%fused_computation.18 | loop fusion | flops 32768 | bytes 200768 | tf_op jit(solution)/shard_map/neg | solution.py:481
  2.0 0.9 fusion.13
  2.8 0.1 pad_maximum_fusion.6
  2.9 0.3 broadcast_multiply_fusion
  3.2 0.9 fusion.12
  4.1 0.1 maximum_multiply_fusion
  4.2 0.8 pad_maximum_fusion.3.qs
  5.0 0.8 pad_maximum_fusion.5.ks
  5.8 0.7 broadcast_multiply_fusion.4
  6.5 0.9 broadcast_multiply_fusion.1
  7.4 0.8 pad_maximum_fusion.1.qc
  8.3 0.8 pad_maximum_fusion.4.kc
  9.1 0.0 copy-done.2
  9.1 0.6 dynamic_slice.3
  9.7 1.2 broadcast_in_dim.16.lam
  10.9 0.0 copy-done.1
  10.9 5.1 %fusion = (f32[3,1024]{1,0:T(4,128)S(1)}, f32[3,1024]{1,0:T(4,128)S(1)}) fusion(bf16[1024,3,1024]{2,0,1:T(8,128)(2,1)} %param.16, f32[1024]{0:T(1024)S(1)} %bitcast.8, f32[1024]{0:T(1024)S(1)} %bitcast.7), kind=kLoop, calls=%fused_computation.2 | loop fusion | flops 15722496 | bytes 6324224 | tf_op jit(solution)/shard_map/reduce_sum | solution.py:470
  16.0 0.1 pad.28.clone
  16.1 0.7 maximum_maximum_fusion.part
  16.8 0.7 compare_convert_fusion.ones_bd
  17.5 0.7 maximum_bitcast_fusion.ckg
  18.1 114.6 %shard_map.127 = bf16[512,1024]{1,0:T(8,128)(2,1)} custom-call(bf16[512,1024]{1,0:T(8,128)(2,1)} %lat.1, bf16[256,1024]{1,0:T(8,128)(2,1)} %ctx.1, f32[8,1024]{1,0:T(8,128)} %maximum_maximum_fusion.part, f32[1,1024]{1,0:T(1,128)} %bitcast.9, bf16[4096,512]{1,0:T(8,128)(2,1)} %wq_h.1, bf16[4096,512]{1,0:T(8,128)(2,1)} %wk_h.1, bf16[4096,512]{1,0:T(8,128)(2,1)} %wv_h.1, ...), custom_call_target="tpu_custom_call" | custom-call | tf_op jit(solution)/shard_map/pallas_call | solution.py:503
  132.7 2.3 %copy.17 = bf16[512,1024]{1,0:T(8,128)(2,1)} copy(bf16[512,1024]{1,0:T(8,128)(2,1)} %shard_map.127) | data formatting | bytes 2097152
  (10 shorter events, 0.1 us)
Async XLA Ops:
  0.0 9.1 %copy-start.2 = (f32[4]{0:T(128)S(1)}, f32[4]{0:T(128)}, u32[]{:S(2)}) copy-start(f32[4]{0:T(128)} %param.23) | copy-start | bytes 52
  0.0 10.9 %copy-start.1 = (f32[2,1024]{1,0:T(2,128)S(1)}, f32[2,1024]{1,0:T(2,128)}, u32[]{:S(2)}) copy-start(f32[2,1024]{1,0:T(2,128)} %param.15) | copy-start | bytes 24580
  0.0 17.5 %copy-start = (f32[64]{0:T(128)S(1)}, f32[64]{0:T(128)}, u32[]{:S(2)}) copy-start(f32[64]{0:T(128)} %param.22) | copy-start | bytes 772

commit v2 on v1

--- a/solution.py
+++ b/solution.py
@@ -3,6 +3,7 @@
 
 import jax
 import jax.numpy as jnp
+import numpy as np
 from jax import lax
 from jax.experimental import pallas as pl
 from jax.experimental.pallas import tpu as pltpu
@@ -186,8 +187,8 @@
 
 
 def fused_kernel(
-    sp, tp, lat, ctx, part, gain, wq_h, wk_h, wv_h, wo_h, qc, qs, kc, ks, ckg, lam, og, ones_bd,
-    out, X, PA, CO, WQ, WK, WV, WO, H, SL, SC, RL, RC, KX, VX, SS, OS, HO,
+    sp, tp, lat, ctx, part, gain, wq_h, wk_h, wv_h, wo_h, qg, kg, rcos, rsin, ccos, csin, lambdas, og,
+    out, X, PA, CO, WQ, WK, WV, WO, H, SL, SC, RL, RC, KX, VX, SS, AC, PK, OS, HO,
     loc_sem, w_sem, xs, xr, ds, dr, fs, fr, ps, pr, cs, cr, zs, zr, os_, or_, gs, gr, es, er, hs, hr,
 ):
     ms = lax.axis_index("sp")
@@ -277,6 +278,33 @@
 
     lane = lax.broadcasted_iota(jnp.int32, (n, 2 * DK), 1)
     low = lax.rem(lane, DK // 2) < DK // 4
+    by_row = lax.rem(lane[:GRID_W], DK) < DK // 2
+    bd_row = lax.broadcasted_iota(jnp.int32, (2 * DK, 2 * DK), 0) < DK
+    bd_col = lax.broadcasted_iota(jnp.int32, (2 * DK, 2 * DK), 1) < DK
+    ones_bd = jnp.where(bd_row == bd_col, 1.0, 0.0).astype(BF)
+
+    def swapped(v):
+        where = low[:v.shape[0]]
+        return jnp.where(where, pltpu.roll(v, 2 * DK - DK // 4, 1), pltpu.roll(v, DK // 4, 1))
+
+    def gains(ref, scale):
+        g = jnp.concatenate([ref[...], ref[...]], axis=1) * scale
+        return g, swapped(jnp.broadcast_to(g, (8, 2 * DK)))[0:1]
+
+    q_gain, q_swap = gains(qg, DK ** (-0.5) * math.log2(math.e))
+    k_gain, k_swap = gains(kg, 1.0)
+    heads_lane = lax.broadcasted_iota(jnp.int32, lambdas.shape, 1)
+    lam = jnp.sum(jnp.where(heads_lane == ms, lambdas[...], 0.0), axis=1, keepdims=True)
+
+    def table(row_ref, col_ref, c):
+        start = ms * (lat.shape[0] // GRID_W) + (c - 1) * (n // GRID_W)
+        return jnp.concatenate(
+            [
+                jnp.where(by_row, row_ref[pl.ds(start + r, 1), :], col_ref[...])
+                for r in range(n // GRID_W)
+            ],
+            axis=0,
+        )
 
     def f_send(c, d):
         ref = X.at[xq[d], pl.ds(c * n, n)]
@@ -291,13 +319,12 @@
 
     def normed(v):
         square = (v * v).astype(BF)
-        mean = jnp.dot(square, ones_bd[...], preferred_element_type=F32)
+        mean = jnp.dot(square, ones_bd, preferred_element_type=F32)
         return v * lax.rsqrt(mean * (1.0 / DK) + epsilon)
 
     def turned(v, ctab, stab):
         w = normed(v)
-        swapped = jnp.where(low, pltpu.roll(w, 2 * DK - DK // 4, 1), pltpu.roll(w, DK // 4, 1))
-        return (w * ctab + swapped * stab).astype(BF)
+        return (w * ctab + swapped(w) * stab).astype(BF)
 
     for c in range(nl + 1):
         rows = pl.ds(c * n, n)
@@ -327,17 +354,19 @@
             weights[2].wait()
         off = 0 if c == 0 else DV
         if c > 0:
-            tr = pl.ds((c - 1) * n, n)
+            cosine, sine = table(rcos, ccos, c), table(rsin, csin, c)
+            qc, qs = cosine * q_gain, sine * q_swap
+            kc, ks = cosine * k_gain, sine * k_swap
             raw = jnp.dot(H[...], WQ[...], preferred_element_type=F32)
             for z in range(sp):
-                SL[z, c - 1, :, 0:DV] = turned(raw[:, z * DV:(z + 1) * DV], qc[tr, :], qs[tr, :])
+                SL[z, c - 1, :, 0:DV] = turned(raw[:, z * DV:(z + 1) * DV], qc, qs)
         raw = jnp.dot(H[...], WK[...], preferred_element_type=F32)
         for z in range(sp):
             piece = raw[:, z * DV:(z + 1) * DV]
             if c == 0:
-                SC[z, :, 0:DV] = (normed(piece) * ckg[...]).astype(BF)
+                SC[z, :, 0:DV] = (normed(piece) * k_gain).astype(BF)
             else:
-                SL[z, c - 1, :, DV:2 * DV] = turned(piece, kc[tr, :], ks[tr, :])
+                SL[z, c - 1, :, DV:2 * DV] = turned(piece, kc, ks)
         raw = jnp.dot(H[...], WV[...], preferred_element_type=F32)
         for z in range(sp):
             piece = raw[:, z * DV:(z + 1) * DV].astype(BF)
@@ -352,13 +381,11 @@
         else:
             RL[ms, c - 1] = SL[ms, c - 1]
 
-    for c in range(nl + 1):
+    def take(c):
         for d in range(sp - 1):
             z_send(c, d).wait()
-    nk = sp * (nl + 1)
-    for s in range(sp):
-        for c in range(nl + 1):
-            kb = s * (nl + 1) + c
+        for s in range(sp):
+            kb = c * sp + s
             if c == 0:
                 KX[kb] = RC[s, :, 0:DV]
                 VX[kb, :, 0:DV] = RC[s, :, DV:2 * DV]
@@ -388,38 +415,89 @@
         ref = HO.at[xq[d], pl.ds(half * n, n)]
         return remote(ref, ref, hs.at[half, d], hr.at[half, d], {"tp": mate})
 
-    def attend(z, half):
+    def stacked(z, half):
         q = RL[z, half, :, 0:DV]
         zero = jnp.zeros_like(q)
-        qq = jnp.concatenate([jnp.where(first, q, zero), jnp.where(first, zero, q)], axis=0)
-        peak = None
-        for kb in range(nk):
-            s = lax.dot_general(qq, KX[kb], (((1,), (1,)), ((), ())), preferred_element_type=F32)
-            SS[kb] = s
-            for j in range(n // 128):
-                piece = s[:, j * 128:(j + 1) * 128]
-                peak = piece if peak is None else jnp.maximum(peak, piece)
-        peak = jnp.max(peak, axis=1, keepdims=True)
-        acc = jnp.zeros((2 * n, 2 * DV), F32)
-        for kb in range(nk):
-            p = jnp.exp2(SS[kb] - peak).astype(BF)
-            acc = acc + jnp.dot(p, VX[kb], preferred_element_type=F32)
+        return jnp.concatenate([jnp.where(first, q, zero), jnp.where(first, zero, q)], axis=0)
+
+    def merge(old, new):
+        peak = jnp.maximum(old[0], new[0])
+        return peak, old[1] * jnp.exp2(old[0] - peak) + new[1] * jnp.exp2(new[0] - peak)
+
+    def attend(zs_here, half, groups, states):
+        queries = [stacked(z, half) for z in zs_here]
+        stages = [(i, g) for i in range(len(zs_here)) for g in groups]
+        peaks = {}
+
+        def score(k, j):
+            i, g = stages[k]
+            s = lax.dot_general(
+                queries[i], KX[g * sp + j], (((1,), (1,)), ((), ())), preferred_element_type=F32
+            )
+            SS[k * sp + j] = s
+            for m in range(n // 128):
+                piece = s[:, m * 128:(m + 1) * 128]
+                peaks[k] = piece if k not in peaks else jnp.maximum(peaks[k], piece)
+
+        for j in range(sp):
+            score(0, j)
+        for k, (i, g) in enumerate(stages):
+            peak = jnp.max(peaks[k], axis=1, keepdims=True)
+            acc = None
+            for j in range(sp):
+                p = jnp.exp2(SS[k * sp + j] - peak).astype(BF)
+                term = jnp.dot(p, VX[g * sp + j], preferred_element_type=F32)
+                acc = term if acc is None else acc + term
+                if k + 1 < len(stages):
+                    score(k + 1, j)
+            states[i] = (peak, acc) if states[i] is None else merge(states[i], (peak, acc))
+        return states
+
+    def finish(state):
+        acc = state[1]
         o = acc[:, :DV] / acc[:, DV:]
-        a = o[:n] - lam[...] * o[n:]
+        a = o[:n] - lam * o[n:]
         a = a * lax.rsqrt(jnp.mean(a * a, axis=1, keepdims=True) + epsilon) * og[...]
         return a.astype(BF)
 
+    per = 2 if sp % 2 == 0 else 1
+
+    def places(i):
+        return [lax.rem(ms + 1 + i * per + e, sp) for e in range(per)]
+
+    early = nl - 1
+    for c in range(nl):
+        take(c)
+
+    def ahead(i, carry):
+        here = places(i)
+        for z, (peak, acc) in zip(here, attend(here, 0, range(nl), [None] * per)):
+            AC[z] = acc
+            PK[z] = jnp.broadcast_to(peak, (2 * n, DV))
+        return carry
+
+    if early:
+        lax.fori_loop(0, sp // per, ahead, 0)
+    take(nl)
+
     for half in range(nl):
         def step(i, carry):
-            z = lax.rem(ms + 1 + i, sp)
-            OS[half, z] = attend(z, half)
-            for d in range(sp - 1):
-                @pl.when(i == d)
-                def _():
-                    o_send(half, d).start()
+            here = places(i)
+            if early and half == 0:
+                states = [(PK[z][:, 0:1], AC[z]) for z in here]
+                states = attend(here, half, [nl], states)
+            else:
+                states = attend(here, half, range(nl + 1), [None] * per)
+            for e, z in enumerate(here):
+                OS[half, z] = finish(states[e])
+                for d in range(sp - 1):
+                    if d % per == e:
+                        @pl.when(i == d // per)
+                        def _():
+                            o_send(half, d).start()
             return carry
 
-        lax.fori_loop(0, sp, step, 0)
+        lax.fori_loop(0, sp // per, step, 0)
         HO[mt, half * n:(half + 1) * n, pl.ds(pl.multiple_of(ms * DV, DV), DV)] = OS[half, ms]
         for d in range(sp - 1):
             o_send(half, d).wait()
@@ -446,17 +524,6 @@
         out[rows, :] = (residual + CO[mt, 4:5, :] * mixed).astype(BF)
 
 
-def swap_lanes(v):
-    quarter = DK // 4
-    return jnp.concatenate(
-        [
-            v[..., quarter:2 * quarter], v[..., :quarter],
-            v[..., 3 * quarter:], v[..., 2 * quarter:3 * quarter],
-        ],
-        axis=-1,
-    )
-
-
 def fused(
     sp, tp, latent, context, conditions, mod_weight, norm_gain, w_query, w_key, w_value,
     query_gain, key_gain, lambdas, out_gain, w_out,
@@ -471,29 +538,18 @@
         + [jnp.zeros((2, cols), F32)],
         axis=0,
     )
-    positions = lax.axis_index("sp") * tok + jnp.arange(tok, dtype=jnp.int32)
-    quarter = DK // 4
-    inverse = 10000.0 ** (-4.0 * jnp.arange(quarter, dtype=F32) / DK)
-    row_angle = (positions // GRID_W).astype(F32)[:, None] * inverse
-    column_angle = (positions % GRID_W).astype(F32)[:, None] * inverse
-    cosine = jnp.concatenate([jnp.cos(row_angle)] * 2 + [jnp.cos(column_angle)] * 2, axis=1)
-    rs, cs = jnp.sin(row_angle), jnp.sin(column_angle)
-    sine = jnp.concatenate([-rs, rs, -cs, cs], axis=1)
-    factor = DK ** (-0.5) * math.log2(math.e)
-
-    def pair(g, scale):
-        c = cosine * (g * scale)
-        s = sine * (swap_lanes(g) * scale)
-        return jnp.concatenate([c, c], axis=1), jnp.concatenate([s, s], axis=1)
-
-    qc, qs = pair(query_gain, factor)
-    kc, ks = pair(key_gain, 1.0)
-    ckg = jnp.concatenate([key_gain, key_gain])[None]
-    lam = jnp.broadcast_to(
-        lax.dynamic_slice_in_dim(lambdas, lax.axis_index("sp"), 1)[None], (1, DV)
-    )
-    which = jnp.arange(2 * DK) // DK
-    ones_bd = (which[:, None] == which[None]).astype(BF)
+    inverse = 10000.0 ** (-4.0 * np.arange(DK // 4) / DK)
+    sign = np.where(np.arange(2 * DK) % (DK // 2) < DK // 4, -1.0, 1.0)
+
+    def trig(count):
+        angles = np.arange(count)[:, None] * np.tile(inverse, 8)[None]
+        return (
+            jnp.asarray(np.cos(angles).astype(np.float32)),
+            jnp.asarray((np.sin(angles) * sign).astype(np.float32)),
+        )
+
+    rcos, rsin = trig(sp * tok // GRID_W)
+    ccos, csin = trig(GRID_W)
     nx = tp // 2
     any_ = pl.BlockSpec(memory_space=pl.ANY)
     vm = pl.BlockSpec(memory_space=pltpu.VMEM)
@@ -520,7 +576,9 @@
             pltpu.VMEM((sp, n, 2 * DV), BF),
             pltpu.VMEM((nk, n, DV), BF),
             pltpu.VMEM((nk, n, 2 * DV), BF),
-            pltpu.VMEM((nk, 2 * n, n), F32),
+            pltpu.VMEM((2 * nk, 2 * n, n), F32),
+            pltpu.VMEM((sp, 2 * n, 2 * DV), F32),
+            pltpu.VMEM((sp, 2 * n, DV), F32),
             pltpu.VMEM((nl, sp, n, DV), BF),
             pltpu.VMEM((tp, tok, sp * DV), BF),
             dma((nl + 1,)),
@@ -541,7 +599,7 @@
         ),
     )(
         latent, context, part, norm_gain[None], w_query, w_key, w_value, w_out,
-        qc, qs, kc, ks, ckg, lam, out_gain[None], ones_bd,
+        query_gain[None], key_gain[None], rcos, rsin, ccos, csin, lambdas[None], out_gain[None],
     )
 
 
@@ -550,7 +608,7 @@
     rows = context.shape[0]
     fits = (
         lambdas.shape[0] == sp and sp > 1 and tp % 2 == 0 and tp > 2
-        and latent.shape[0] % rows == 0 and rows % 128 == 0 and rows <= 256
+        and latent.shape[0] % rows == 0 and rows % 128 == 0 and rows <= 256 and rows % GRID_W == 0
         and latent.shape[0] <= 2 * rows and latent.shape[1] % 128 == 0
         and latent.shape[1] <= 1024 and tp <= 4
     )

time: 135 us -> 112 us (0.83)
  Pallas kernels: 115 us -> 103 us
  other arithmetic: 14.5 us -> 6.34 us
  local copies, waits for them, and re-layouts: 5.86 us -> 2.35 us
    pallas_call x1, Pallas kernels: 115 us -> 103 us  [fused(): pl.pallas_call(functools.partial(fused_kernel, sp, tp), out_shape=jax.Sha...]
    concatenate x5 -> x0, other arithmetic: 3.42 us -> none  [the longest x4 3.35 us: pair(): return (jnp.concatenate([c, c], axis=1), jnp.concatenate([s, s], axis=1))]
    mul x5 -> x0, other arithmetic: 1.96 us -> none  [the longest x2 1.58 us: pair(): c = cosine * (g * scale)]
    neg x1 -> x0, other arithmetic: 1.9 us -> none  [fused(): sine = jnp.concatenate([-rs, rs, -cs, cs], axis=1)]
    slice x2 -> x0, local copies, waits for them, and re-layouts: 1.75 us -> none  [swap_lanes(): v[..., quarter:2 * quarter]]
where the time goes in v2:
time: 112 us
  Pallas kernels  103 us (92%)
  other arithmetic  6.34 us (6%)
  local copies, waits for them, and re-layouts  2.35 us (2%)
    pallas_call x1, Pallas kernels, fused(): pl.pallas_call(functools.partial(fused_kernel, sp, tp), out_shape=jax.Sha...  103 us
    reduce_sum x1, other arithmetic, fused(): jnp.sum(weight * activated[c][:, None, None], axis=0)  4.94 us
    unnamed x1, local copies, waits for them, and re-layouts  2.26 us

profile of v2, /device:TPU:0, one launch (start us, length us, event | category | flops | bytes accessed | tf_op | source)
XLA Modules:
  0.0 111.7 jit_solution(16036569922139705019)
XLA Ops:
  0.0 0.1 pad.2.clone
  0.1 0.7 fusion.3
  0.8 4.9 %fusion = (f32[3,1024]{1,0:T(4,128)S(1)}, f32[3,1024]{1,0:T(4,128)S(1)}) fusion(bf16[1024,3,1024]{2,0,1:T(8,128)(2,1)} %param.20, f32[1024]{0:T(1024)S(1)} %bitcast.8, f32[1024]{0:T(1024)S(1)} %bitcast.7), kind=kLoop, calls=%fused_computation.2 | loop fusion | flops 15722496 | bytes 6324224 | tf_op jit(solution)/shard_map/reduce_sum | solution.py:537
  5.8 0.7 maximum_maximum_fusion.part
  6.4 103.0 %shard_map.163 = bf16[512,1024]{1,0:T(8,128)(2,1)} custom-call(bf16[512,1024]{1,0:T(8,128)(2,1)} %lat.1, bf16[256,1024]{1,0:T(8,128)(2,1)} %ctx.1, f32[8,1024]{1,0:T(8,128)} %maximum_maximum_fusion.part, f32[1,1024]{1,0:T(1,128)} %bitcast.9, bf16[4096,512]{1,0:T(8,128)(2,1)} %wq_h.1, bf16[4096,512]{1,0:T(8,128)(2,1)} %wk_h.1, bf16[4096,512]{1,0:T(8,128)(2,1)} %wv_h.1, ...), custom_call_target="tpu_custom_call" | custom-call | tf_op jit(solution)/shard_map/pallas_call | solution.py:559
  109.4 2.3 %copy.19 = bf16[512,1024]{1,0:T(8,128)(2,1)} copy(bf16[512,1024]{1,0:T(8,128)(2,1)} %shard_map.163) | data formatting | bytes 2097152
  (2 shorter events, 0.0 us)
